TPU v7x, 32 devices: a whole 2x2x4 slice. The times are simulated.
32 devices in a mesh: ep: 4 (over y, x), tp: 8 (over z, core).
Axes of the slice: x: 2, y: 2, z: 4, core: 2. Of those that a mesh axis runs over, the one named last changes fastest.
Arguments:
- tokens: bfloat16 [64, 2048], P('ep', 'tp'), may hold values from -6 to 6
- key_cache: bfloat16 [64, 16, 1024, 128], P('ep', 'tp'), may hold values from -1700 to 1700
- value_cache: bfloat16 [64, 16, 1024, 128], P('ep', 'tp'), may hold values from -6 to 6
- gate_totals: float32 [64, 16, 1024], P('ep', 'tp'), as said below
- lengths: int32 [64], P('ep'), may hold values from 128 to 1024
- attn_gain: float32 [2048], replicated, may hold values from 0.1 to 1.9
- w_query: bfloat16 [2048, 2048], P(None, 'tp'), may hold values from -0.125 to 0.125
- w_key: bfloat16 [2048, 2048], P(None, 'tp'), may hold values from -0.125 to 0.125
- w_value: bfloat16 [2048, 2048], P(None, 'tp'), may hold values from -0.125 to 0.125
- w_forget: bfloat16 [2048, 16], replicated, may hold values from -0.125 to 0.125
- forget_bias: float32 [16], replicated, may hold values from -3 to 0
- w_attn_out: bfloat16 [2048, 2048], P('tp'), may hold values from -0.1875 to 0.1875
- moe_gain: float32 [2048], replicated, may hold values from 0.1 to 1.9
- group_ids: int32 [64, 1], P('ep'), may hold values from 0 to 3; in each aligned block of 16 rows (0 to 15, 16 to 31, ...) at most 8 rows name the same one
- inner_ids: int32 [64, 2], P('ep'), may hold values from 0 to 3, all different within a row
- group_prob: float32 [64], P('ep'), may hold values from 0.2 to 1
- pair_logits: float32 [64, 2], P('ep'), may hold values from -6 to 6
- w_expert_gate: bfloat16 [4, 2048, 2048], P('ep', None, 'tp'), may hold values from -0.125 to 0.125
- w_expert_up: bfloat16 [4, 2048, 2048], P('ep', None, 'tp'), may hold values from -0.125 to 0.125
- w_expert_down: bfloat16 [4, 2048, 2048], P('ep', 'tp'), may hold values from -0.375 to 0.375
- w_dense_in: bfloat16 [2048, 2048], P(None, 'tp'), may hold values from -0.125 to 0.125
- w_dense_out: bfloat16 [2048, 2048], P('tp'), may hold values from -0.1875 to 0.1875
- dense_gate: float32 [2048], P('tp'), may hold values from -2 to 2
Outputs:
- layer_output: bfloat16 [64, 2048], P('ep', 'tp')
- new_keys: bfloat16 [64, 16, 128], P('ep', 'tp')
- new_values: bfloat16 [64, 16, 128], P('ep', 'tp')
- new_gates: float32 [64, 16], P('ep', 'tp')
Inputs may be any that keep to these rules, and one draw needn't show every extreme that they name: `group_ids`: within the 16 sequences of each index of ep (aligned blocks of rows), no group is named by more than 8 sequences, a bound that some block reaches. `inner_ids`: each row names 2 different experts of its group. `gate_totals`: along positions the values of each sequence and head never rise.
All inputs are finite; a program needn't handle non-finite values.
Results may differ from a plain program's by a relative error of at most 0.011.
Values may be sent and summed in bfloat16 or wider, within the bound.
A program may use at most 64 MiB of HBM per device.

v0:
```python
import jax
import jax.numpy as jnp
from jax import lax
from jax.sharding import PartitionSpec as P

FFE = 512
EPG = 4
EPS = 1e-06
FLOOR = -1e30


def norm_rows(row_data, gain_vec):
    values = row_data.astype(jnp.float32)
    factor = lax.rsqrt(jnp.mean(values * values, axis=-1, keepdims=True) + EPS)
    return (values * factor * gain_vec).astype(jnp.bfloat16)


def head_norm(values):
    factor = lax.rsqrt(jnp.mean(values * values, axis=-1, keepdims=True) + EPS)
    return (values * factor).astype(jnp.bfloat16)


def attend(queries, fresh_key, fresh_value, key_cache, value_cache, gate_totals, lengths, current):
    score_scale = queries.shape[-1] ** (-0.5)
    scores = (
        jnp.einsum("shd,shld->shl", queries, key_cache, preferred_element_type=jnp.float32)
        * score_scale
    )
    scores = scores + current[:, :, None] - gate_totals
    entry_indices = jnp.arange(key_cache.shape[2])
    live_mask = (entry_indices[None, :] < lengths[:, None])[:, None, :]
    scores = jnp.where(live_mask, scores, FLOOR)
    own_score = (
        jnp.sum(queries.astype(jnp.float32) * fresh_key.astype(jnp.float32), axis=-1) * score_scale
    )
    peak = jnp.maximum(jnp.max(scores, axis=-1), own_score)
    expo_terms = jnp.where(live_mask, jnp.exp(scores - peak[:, :, None]), 0.0)
    own_expo = jnp.exp(own_score - peak)
    denom_sum = jnp.sum(expo_terms, axis=-1) + own_expo
    weights = (expo_terms / denom_sum[:, :, None]).astype(jnp.bfloat16)
    own_weight = (own_expo / denom_sum).astype(jnp.bfloat16)
    attended = jnp.einsum("shl,shld->shd", weights, value_cache, preferred_element_type=jnp.float32)
    attended = attended + own_weight.astype(jnp.float32)[:, :, None] * fresh_value.astype(
        jnp.float32
    )
    return attended.astype(jnp.bfloat16)


def body(
    tokens,
    key_cache,
    value_cache,
    gate_totals,
    lengths,
    attn_gain,
    w_query,
    w_key,
    w_value,
    w_forget,
    forget_bias,
    w_attn_out,
    moe_gain,
    group_ids,
    inner_ids,
    group_prob,
    pair_logits,
    w_expert_gate,
    w_expert_up,
    w_expert_down,
    w_dense_in,
    w_dense_out,
    dense_gate,
):
    gathered = lax.all_gather(tokens, "tp", axis=1, tiled=True)
    normed = norm_rows(gathered, attn_gain)
    seq_count = gathered.shape[0]
    heads_dev = key_cache.shape[1]
    head_dim = key_cache.shape[3]

    def project(weight):
        return jnp.dot(normed, weight, preferred_element_type=jnp.float32).reshape(
            seq_count, heads_dev, head_dim
        )

    queries = head_norm(project(w_query))
    new_keys = head_norm(project(w_key))
    new_values = project(w_value).astype(jnp.bfloat16)
    first_head = lax.axis_index("tp") * heads_dev
    forget_cols = lax.dynamic_slice_in_dim(w_forget, first_head, heads_dev, 1)
    forget_shift = lax.dynamic_slice_in_dim(forget_bias, first_head, heads_dev, 0)
    log_gate = jax.nn.log_sigmoid(
        jnp.dot(normed, forget_cols, preferred_element_type=jnp.float32) + forget_shift
    )
    entry_indices = jnp.arange(gate_totals.shape[2])
    at_last = (entry_indices[None, :] == (lengths - 1)[:, None])[:, None, :]
    new_gates = jnp.sum(jnp.where(at_last, gate_totals, 0.0), axis=2) + log_gate
    attended = attend(
        queries, new_keys, new_values, key_cache, value_cache, gate_totals, lengths, new_gates
    )
    partial_value = jnp.dot(
        attended.reshape(seq_count, heads_dev * head_dim),
        w_attn_out,
        preferred_element_type=jnp.float32,
    )
    piece_sum = lax.psum_scatter(partial_value, "tp", scatter_dimension=1, tiled=True)
    own_residual = (tokens.astype(jnp.float32) + piece_sum).astype(jnp.bfloat16)
    moe_in = norm_rows(lax.all_gather(own_residual, "tp", axis=1, tiled=True), moe_gain)
    groups = lax.axis_size("ep")
    capacity = max(2, 2 * seq_count // groups)
    first_share = jax.nn.sigmoid(pair_logits[:, 0] - pair_logits[:, 1])
    pair_share = group_prob[:, None] * jnp.stack([first_share, 1.0 - first_share], axis=1)
    inner_range = jnp.arange(EPG)
    spread = jnp.sum(
        jnp.where(inner_ids[:, :, None] == inner_range[None, None, :], pair_share[:, :, None], 0.0),
        axis=1,
    ).astype(jnp.bfloat16)
    choose = (group_ids == jnp.arange(groups)[None, :]).astype(jnp.int32)
    before = jnp.cumsum(choose, axis=0) - choose
    slot_of = group_ids[:, 0] * capacity + jnp.sum(before * choose, axis=1)
    slot_ids = jnp.arange(groups * capacity)
    send_map = (slot_of[None, :] == slot_ids[:, None]).astype(jnp.bfloat16)
    send_weights = jnp.dot(send_map, spread, preferred_element_type=jnp.float32).astype(
        jnp.bfloat16
    )
    send_rows = jnp.dot(send_map, moe_in, preferred_element_type=jnp.float32).astype(jnp.bfloat16)
    recv_rows, recv_weights = (
        lax.all_to_all(send_rows, "ep", split_axis=0, concat_axis=0, tiled=True),
        lax.all_to_all(send_weights, "ep", split_axis=0, concat_axis=0, tiled=True),
    )
    dense_hidden = jax.nn.silu(
        jnp.dot(moe_in, w_dense_in, preferred_element_type=jnp.float32)
    ).astype(jnp.bfloat16)
    dense_part = jnp.dot(dense_hidden, w_dense_out, preferred_element_type=jnp.float32)
    hidden_dev = w_expert_gate.shape[2]
    expert_index = lax.axis_index("tp") * hidden_dev // FFE
    route_col = jnp.sum(
        jnp.where(inner_range[None, :] == expert_index, recv_weights.astype(jnp.float32), 0.0),
        axis=1,
    )
    gate_pre = jnp.dot(recv_rows, w_expert_gate[0], preferred_element_type=jnp.float32)
    up_pre = jnp.dot(recv_rows, w_expert_up[0], preferred_element_type=jnp.float32)
    hidden = (jax.nn.silu(gate_pre) * up_pre * route_col[:, None]).astype(jnp.bfloat16)
    expert_part = jnp.dot(hidden, w_expert_down[0], preferred_element_type=jnp.float32)
    expert_sum, dense_sum = (
        lax.psum_scatter(expert_part, "tp", scatter_dimension=1, tiled=True),
        lax.psum_scatter(dense_part, "tp", scatter_dimension=1, tiled=True),
    )
    returned = lax.all_to_all(
        expert_sum.astype(jnp.bfloat16), "ep", split_axis=0, concat_axis=0, tiled=True
    )
    expert_out = lax.dot_general(
        send_map, returned, (((0,), (0,)), ((), ())), preferred_element_type=jnp.float32
    )
    layer_output = (
        own_residual.astype(jnp.float32) + expert_out + jax.nn.sigmoid(dense_gate) * dense_sum
    )
    return (layer_output.astype(jnp.bfloat16), new_keys, new_values, new_gates)


def solution(mesh):
    placed = (
        P("ep", "tp"),
        P("ep", "tp", None, None),
        P("ep", "tp", None, None),
        P("ep", "tp", None),
        P("ep"),
        P(),
        P(None, "tp"),
        P(None, "tp"),
        P(None, "tp"),
        P(),
        P(),
        P("tp", None),
        P(),
        P("ep", None),
        P("ep", None),
        P("ep"),
        P("ep", None),
        P("ep", None, "tp"),
        P("ep", None, "tp"),
        P("ep", "tp", None),
        P(None, "tp"),
        P("tp", None),
        P("tp"),
    )
    return jax.shard_map(
        body,
        mesh=mesh,
        in_specs=placed,
        out_specs=(P("ep", "tp"), P("ep", "tp", None), P("ep", "tp", None), P("ep", "tp")),
        check_vma=False,
    )
```

profile of v0, /device:TPU:0, one launch (start us, length us, event | category | flops | bytes accessed | tf_op | source)
XLA Modules:
  0.0 172.8 jit_solution(14352880859179264883)
XLA Ops:
  7.3 0.8 broadcast_add_fusion
  8.1 0.7 iota_compare_fusion.1
  8.8 15.9 %all_gather.6 = bf16[16,2048]{1,0:T(8,128)(2,1)S(1)} all-gather(bf16[16,256]{1,0:T(8,128)(2,1)} %param.23), channel_id=1, replica_groups=mesh['ep'=4,'tp'=8] {'tp'}, dimensions={1}, use_global_device_ids=true | all-gather | bytes 73728 | tf_op jit(solution)/shard_map/all_gather | solution.py:74
  24.8 1.5 fusion.67
  26.5 1.5 fusion.70
  28.2 1.1 select_reduce_fusion
  30.1 1.0 fusion.58
  31.9 5.6 %fusion.34 = f32[16,2,1,1024]{3,2,1,0:T(1,128)S(1)} fusion(bf16[16,2,1024,128]{3,2,1,0:T(8,128)(2,1)} %param.24, bf16[16,2,128,1]{2,1,0,3:T(2,128)(2,1)S(1)} %get-tuple-element.12), kind=kOutput, calls=%fused_computation.48 | convolution fusion | flops 8388608 | bytes 8527872 | tf_op jit(solution)/shard_map/shd,shld->shl/dot_general | solution.py:26
  38.9 4.7 %fusion.24 = f32[16,2,1,128]{3,2,1,0:T(1,128)S(1)} fusion(bf16[16,2,1024,128]{3,2,1,0:T(8,128)(2,1)} %param.25, bf16[16,2,1024,1]{2,1,0,3:T(2,128)(2,1)S(1)} %fusion.26), kind=kOutput, calls=%fused_computation.33 | convolution fusion | flops 8388608 | bytes 8470528 | tf_op jit(solution)/shard_map/shl,shld->shd/dot_general | solution.py:42
  43.7 2.1 %fusion.46 = f32[16,2048]{1,0:T(8,128)} fusion(bf16[256,2048]{1,0:T(8,128)(2,1)} %param.34, bf16[2,8,2,128]{3,2,1,0:T(2,128)(2,1)S(1)} %bitcast.56), kind=kOutput, calls=%fused_computation.66 | convolution fusion | flops 16777216 | bytes 1187840 | tf_op jit(solution)/shard_map/dot_general | solution.py:100
  47.0 3.7 %all-to-all-start.1 = ((bf16[4,8,4]{1,2,0:T(4,128)(2,1)}), bf16[4,8,4]{1,2,0:T(4,128)(2,1)S(1)}, u32[]{:S(2)}, u32[]{:S(2)}) async-start(bf16[4,8,4]{1,2,0:T(4,128)(2,1)} %copy.49), calls=%async_computation.2 | async-start | bytes 8192 | tf_op jit(solution)/shard_map/all_to_all | solution.py:128
  50.8 26.8 %reduce-scatter.4.cloned.1.call-done = f32[16,256]{1,0:T(8,128)} async-done(((f32[16,2048]{1,0:T(8,128)}), f32[16,256]{1,0:T(8,128)}) %reduce-scatter.4.cloned.1.call-update) | async-done | bytes 16400 | tf_op jit(solution)/shard_map/reduce_scatter | solution.py:105
  78.3 13.9 %all_gather.7 = bf16[16,2048]{1,0:T(8,128)(2,1)S(1)} all-gather(bf16[16,256]{1,0:T(8,128)(2,1)S(1)} %add_convert_fusion), channel_id=1, replica_groups=mesh['ep'=4,'tp'=8] {'tp'}, dimensions={1}, use_global_device_ids=true | all-gather | bytes 73728 | tf_op jit(solution)/shard_map/all_gather | solution.py:107
  92.4 0.9 fusion
  93.2 3.6 %all-to-all-start = ((bf16[4,8,2048]{2,1,0:T(8,128)(2,1)}), bf16[4,8,2048]{2,1,0:T(8,128)(2,1)S(1)}, u32[]{:S(2)}, u32[]{:S(2)}) async-start(bf16[4,8,2048]{2,1,0:T(8,128)(2,1)} %fusion), calls=%async_computation.1 | async-start | bytes 262144 | tf_op jit(solution)/shard_map/all_to_all | solution.py:127
  97.1 4.8 %all-to-all-done = bf16[4,8,2048]{2,1,0:T(8,128)(2,1)S(1)} async-done(((bf16[4,8,2048]{2,1,0:T(8,128)(2,1)}), bf16[4,8,2048]{2,1,0:T(8,128)(2,1)S(1)}, u32[]{:S(2)}, u32[]{:S(2)}) %all-to-all-start) | async-done | bytes 131104 | tf_op jit(solution)/shard_map/all_to_all | solution.py:127
  101.9 1.5 fusion.10
  103.4 2.7 %fusion.4 = f32[32,2048]{1,0:T(8,128)} fusion(bf16[1,256,2048]{2,1,0:T(8,128)(2,1)S(1)} %copy-done, bf16[1,2048,256]{2,1,0:T(8,128)(2,1)} %param.41, bf16[4,8,2048]{2,1,0:T(8,128)(2,1)S(1)} %all-to-all-done, f32[32,256]{1,0:T(8,128)S(1)} %fusion.10, f32[32]{0:T(128)S(1)} %mul.181), kind=kOutput, calls=%fused_computation.7 | convolution fusion | flops 67166208 | bytes 2523264 | tf_op jit(solution)/shard_map/dot_general | solution.py:143
  106.2 1.5 fusion.44
  107.7 26.1 %reduce-scatter.6.cloned.1.call-done = f32[32,256]{1,0:T(8,128)} async-done(((f32[32,2048]{1,0:T(8,128)}), f32[32,256]{1,0:T(8,128)}) %reduce-scatter.6.cloned.1.call-update) | async-done | bytes 32784 | tf_op jit(solution)/shard_map/reduce_scatter | solution.py:145
  133.7 1.4 convert_bitcast_fusion
  135.1 3.6 %all-to-all-start.2 = ((bf16[4,8,256]{2,1,0:T(8,128)(2,1)}), bf16[4,8,256]{2,1,0:T(8,128)(2,1)S(1)}, u32[]{:S(2)}, u32[]{:S(2)}) async-start(bf16[4,8,256]{2,1,0:T(8,128)(2,1)} %convert_bitcast_fusion), calls=%async_computation.4 | async-start | bytes 32768 | tf_op jit(solution)/shard_map/all_to_all | solution.py:148
  138.7 26.0 %reduce-scatter.8.cloned.1.call-done = f32[16,256]{1,0:T(8,128)} async-done(((f32[16,2048]{1,0:T(8,128)}), f32[16,256]{1,0:T(8,128)}) %reduce-scatter.8.cloned.1.call-update) | async-done | bytes 16400 | tf_op jit(solution)/shard_map/reduce_scatter | solution.py:146
  164.7 1.5 fusion.5
  (75 shorter events, 5.7 us)
Async XLA Ops:
  7.2 96.2 %copy-start = (bf16[1,256,2048]{2,1,0:T(8,128)(2,1)S(1)}, bf16[1,256,2048]{2,1,0:T(8,128)(2,1)}, u32[]{:S(2)}) copy-start(bf16[1,256,2048]{2,1,0:T(8,128)(2,1)} %param.42) | copy-start | bytes 3145732
  7.2 31.3 %copy-start.5 = (f32[2048]{0:T(1024)S(1)}, f32[2048]{0:T(1024)}, u32[]{:S(2)}) copy-start(f32[2048]{0:T(1024)} %param.28) | copy-start | bytes 24580
  7.2 30.3 %copy-start.4 = (f32[16,2,1024]{2,1,0:T(2,128)S(1)}, f32[16,2,1024]{2,1,0:T(2,128)}, u32[]{:S(2)}) copy-start(f32[16,2,1024]{2,1,0:T(2,128)} %param.26) | copy-start | bytes 393220
  7.2 31.3 %copy-start.3 = (bf16[2048,256]{1,0:T(8,128)(2,1)S(1)}, bf16[2048,256]{1,0:T(8,128)(2,1)}, u32[]{:S(2)}) copy-start(bf16[2048,256]{1,0:T(8,128)(2,1)} %param.31) | copy-start | bytes 3145732
  7.2 70.3 %reduce-scatter.4.cloned.1.call-start = ((), (), s32[]{:S(2)}) async-start(), calls=%async_computation.6 | async-start | bytes 147456 | tf_op jit(solution)/shard_map/reduce_scatter | solution.py:105
  31.1 12.5 %copy-start.11 = (f32[16,2]{0,1:T(2,128)}, f32[16,2]{0,1:T(2,128)S(1)}, u32[]{:S(2)}) copy-start(f32[16,2]{0,1:T(2,128)S(1)} %fusion.58) | copy-start | bytes 388
  37.5 8.3 %copy-start.9 = (s32[16,1]{0,1:T(1,128)S(1)}, s32[16,1]{0,1:T(1,128)}, u32[]{:S(2)}) copy-start(s32[16,1]{0,1:T(1,128)} %param.36) | copy-start | bytes 196
  37.5 8.6 %copy-start.12 = (f32[16,2]{0,1:T(2,128)S(1)}, f32[16,2]{0,1:T(2,128)}, u32[]{:S(2)}) copy-start(f32[16,2]{0,1:T(2,128)} %param.39) | copy-start | bytes 388
  37.6 8.6 %copy-start.14 = (f32[16]{0:T(128)S(1)}, f32[16]{0:T(128)}, u32[]{:S(2)}) copy-start(f32[16]{0:T(128)} %param.38) | copy-start | bytes 196
  37.6 8.6 %copy-start.10 = (s32[16,2]{0,1:T(2,128)S(1)}, s32[16,2]{0,1:T(2,128)}, u32[]{:S(2)}) copy-start(s32[16,2]{0,1:T(2,128)} %param.37) | copy-start | bytes 388
  37.6 40.0 %copy-start.8 = (bf16[16,256]{1,0:T(8,128)(2,1)S(1)}, bf16[16,256]{1,0:T(8,128)(2,1)}, u32[]{:S(2)}) copy-start(bf16[16,256]{1,0:T(8,128)(2,1)} %param.23) | copy-start | bytes 24580
  37.6 54.8 %copy-start.6 = (f32[2048]{0:T(1024)S(1)}, f32[2048]{0:T(1024)}, u32[]{:S(2)}) copy-start(f32[2048]{0:T(1024)} %param.35) | copy-start | bytes 24580
  38.8 67.3 %copy-start.7 = (bf16[16,2,128]{2,1,0:T(2,128)(2,1)}, bf16[16,2,128]{2,1,0:T(2,128)(2,1)S(1)}, u32[]{:S(2)}) copy-start(bf16[16,2,128]{2,1,0:T(2,128)(2,1)S(1)} %convert_element_type.102) | copy-start | bytes 24580
  38.8 67.3 %copy-start.1 = (bf16[256,2048]{1,0:T(8,128)(2,1)S(1)}, bf16[256,2048]{1,0:T(8,128)(2,1)}, u32[]{:S(2)}) copy-start(bf16[256,2048]{1,0:T(8,128)(2,1)} %param.44) | copy-start | bytes 3145732
  38.8 67.3 %copy-start.2 = (bf16[2048,256]{1,0:T(8,128)(2,1)S(1)}, bf16[2048,256]{1,0:T(8,128)(2,1)}, u32[]{:S(2)}) copy-start(bf16[2048,256]{1,0:T(8,128)(2,1)} %param.43) | copy-start | bytes 3145732
  38.9 99.9 %copy-start.13 = (f32[256]{0:T(256)S(1)}, f32[256]{0:T(256)}, u32[]{:S(2)}) copy-start(f32[256]{0:T(256)} %param.45) | copy-start | bytes 3076
  47.0 46.2 %all-to-all-start.1 = ((bf16[4,8,4]{1,2,0:T(4,128)(2,1)}), bf16[4,8,4]{1,2,0:T(4,128)(2,1)S(1)}, u32[]{:S(2)}, u32[]{:S(2)}) async-start(bf16[4,8,4]{1,2,0:T(4,128)(2,1)} %copy.49), calls=%async_computation.2 | async-start | bytes 8192 | tf_op jit(solution)/shard_map/all_to_all | solution.py:128
  93.2 8.7 %all-to-all-start = ((bf16[4,8,2048]{2,1,0:T(8,128)(2,1)}), bf16[4,8,2048]{2,1,0:T(8,128)(2,1)S(1)}, u32[]{:S(2)}, u32[]{:S(2)}) async-start(bf16[4,8,2048]{2,1,0:T(8,128)(2,1)} %fusion), calls=%async_computation.1 | async-start | bytes 262144 | tf_op jit(solution)/shard_map/all_to_all | solution.py:127
  96.9 36.9 %reduce-scatter.6.cloned.1.call-start = ((), (), s32[]{:S(2)}) async-start(), calls=%async_computation.7 | async-start | bytes 294912 | tf_op jit(solution)/shard_map/reduce_scatter | solution.py:145
  106.1 58.6 %reduce-scatter.8.cloned.1.call-start = ((), (), s32[]{:S(2)}) async-start(), calls=%async_computation.8 | async-start | bytes 147456 | tf_op jit(solution)/shard_map/reduce_scatter | solution.py:146
  135.1 29.6 %all-to-all-start.2 = ((bf16[4,8,256]{2,1,0:T(8,128)(2,1)}), bf16[4,8,256]{2,1,0:T(8,128)(2,1)S(1)}, u32[]{:S(2)}, u32[]{:S(2)}) async-start(bf16[4,8,256]{2,1,0:T(8,128)(2,1)} %convert_bitcast_fusion), calls=%async_computation.4 | async-start | bytes 32768 | tf_op jit(solution)/shard_map/all_to_all | solution.py:148
Sparse Core Ops, SparseCore 0:
  45.9 31.5 reduce-scatter.3
  106.2 27.4 reduce-scatter.5
  136.0 28.7 reduce-scatter.7
where the time goes:
time: 174 us; the launch traced here: 173 us
  waiting for transfers between devices  83.8 us (48%)
  blocking collectives  29.8 us (17%)
  matrix products  24.9 us (14%)
  between operations  14 us (8%)
  starting transfers between devices  11 us (6%)
  other arithmetic  7.35 us (4%)
  local copies, waits for them, and re-layouts  1.82 us (1%)
    reduce_scatter x1, waiting for transfers between devices, body(): lax.psum_scatter(partial_value, 'tp', scatter_dimension=1, tiled=True)  26.8 us
    reduce_scatter x1, waiting for transfers between devices, body(): lax.psum_scatter(expert_part, 'tp', scatter_dimension=1, tiled=True)  26.1 us
    reduce_scatter x1, waiting for transfers between devices, body(): lax.psum_scatter(dense_part, 'tp', scatter_dimension=1, tiled=True)  26 us
    all_gather x1, blocking collectives, body(): gathered = lax.all_gather(tokens, 'tp', axis=1, tiled=True)  15.9 us
    all_gather x1, blocking collectives, body(): lax.all_gather(own_residual, 'tp', axis=1, tiled=True)  13.9 us
    dot_general x1, matrix products, attend(): jnp.einsum('shd,shld->shl', queries, key_cache, preferred_element_type=jn...  5.63 us
    all_to_all x1, waiting for transfers between devices, body(): lax.all_to_all(send_rows, 'ep', split_axis=0, concat_axis=0, tiled=True)  4.85 us
    dot_general x1, matrix products, attend(): jnp.einsum('shl,shld->shd', weights, value_cache, preferred_element_type=...  4.72 us
  transfers between devices with their start and end apart: 6, of which 4 were waited for; matrix products, arithmetic and copies ran while one was open for 3% of the time, Pallas kernels for 0%

commit v1 on v0

--- a/solution.py
+++ b/solution.py
@@ -7,6 +7,32 @@
 EPG = 4
 EPS = 1e-06
 FLOOR = -1e30
+
+
+def play_weights_over_axis(slab_in, mesh_dim, row_dim):
+    nd = jax.lax.axis_size(mesh_dim)
+    items = []
+    ii = 0
+    while ii < nd:
+        items.append((ii, (ii + 1) % nd))
+        ii = ii + 1
+    sides = []
+    ii = 0
+    while ii < nd:
+        sides.append((ii, (ii - 1) % nd))
+        ii = ii + 1
+    parts_out, x_new = ([slab_in], [slab_in])
+    for _ in range(nd // 2):
+        parts_out.append(jax.lax.ppermute(parts_out[-1], mesh_dim, items))
+    w = 0
+    while w < (nd - 1) // 2:
+        x_new.append(jax.lax.ppermute(x_new[-1], mesh_dim, perm=sides))
+        w = w + 1
+    return jnp.roll(
+        jnp.concatenate([*parts_out[::-1], *x_new[1:]], axis=row_dim),
+        (jax.lax.axis_index(mesh_dim) - nd // 2) * slab_in.shape[row_dim],
+        axis=row_dim,
+    )
 
 
 def norm_rows(row_data, gain_vec):
@@ -104,7 +130,7 @@
     )
     piece_sum = lax.psum_scatter(partial_value, "tp", scatter_dimension=1, tiled=True)
     own_residual = (tokens.astype(jnp.float32) + piece_sum).astype(jnp.bfloat16)
-    moe_in = norm_rows(lax.all_gather(own_residual, "tp", axis=1, tiled=True), moe_gain)
+    moe_in = norm_rows(play_weights_over_axis(own_residual, "tp", 1), moe_gain)
     groups = lax.axis_size("ep")
     capacity = max(2, 2 * seq_count // groups)
     first_share = jax.nn.sigmoid(pair_logits[:, 0] - pair_logits[:, 1])

time: 174 us -> 183 us (1.052)
  blocking collectives: 29.8 us -> 15.9 us
  waiting for transfers between devices: 83.8 us -> 97.2 us
  starting transfers between devices: 11 us -> 21.6 us
    all_gather x1 -> x0, blocking collectives: 13.9 us -> none  [body(): lax.all_gather(own_residual, 'tp', axis=1, tiled=True)]
    ppermute x0 -> x7, starting transfers between devices: none -> 10.4 us  [the longest x3 10.4 us: play_weights_over_axis(): x_new.append(jax.lax.ppermute(x_new[-1], mesh_dim, perm=sides))]
    ppermute x0 -> x7, waiting for transfers between devices: none -> 8.76 us  [the longest x4 6.12 us: play_weights_over_axis(): parts_out.append(jax.lax.ppermute(parts_out[-1], mesh_dim, items))]
    reduce_scatter x1, waiting for transfers between devices: 26.8 us -> 31.4 us  [body(): lax.psum_scatter(partial_value, 'tp', scatter_dimension=1, tiled=True)]
  transfers between devices with their start and end apart: 6 -> 13, of which waited for: 4 -> 8; matrix products, arithmetic and copies ran while one was open for 3% -> 4% of each run, Pallas kernels for 0% -> 0%
where the time goes in v1:
time: 183 us; the launch traced here: 182 us
  waiting for transfers between devices  97.2 us (53%)
  matrix products  23.9 us (13%)
  starting transfers between devices  21.6 us (12%)
  blocking collectives  15.9 us (9%)
  between operations  14.1 us (8%)
  other arithmetic  7.3 us (4%)
  local copies, waits for them, and re-layouts  1.85 us (1%)
    reduce_scatter x1, waiting for transfers between devices, body(): lax.psum_scatter(partial_value, 'tp', scatter_dimension=1, tiled=True)  31.4 us
    reduce_scatter x1, waiting for transfers between devices, body(): lax.psum_scatter(expert_part, 'tp', scatter_dimension=1, tiled=True)  26.1 us
    reduce_scatter x1, waiting for transfers between devices, body(): lax.psum_scatter(dense_part, 'tp', scatter_dimension=1, tiled=True)  26 us
    all_gather x1, blocking collectives, body(): gathered = lax.all_gather(tokens, 'tp', axis=1, tiled=True)  15.9 us
    ppermute x3, starting transfers between devices, play_weights_over_axis(): x_new.append(jax.lax.ppermute(x_new[-1], mesh_dim, perm=sides))  10.4 us
    ppermute x4, waiting for transfers between devices, play_weights_over_axis(): parts_out.append(jax.lax.ppermute(parts_out[-1], mesh_dim, items))  6.12 us
    dot_general x1, matrix products, attend(): jnp.einsum('shd,shld->shl', queries, key_cache, preferred_element_type=jn...  5.63 us
    all_to_all x1, waiting for transfers between devices, body(): lax.all_to_all(send_rows, 'ep', split_axis=0, concat_axis=0, tiled=True)  4.85 us
  transfers between devices with their start and end apart: 13, of which 8 were waited for; matrix products, arithmetic and copies ran while one was open for 4% of the time, Pallas kernels for 0%

profile of v1, /device:TPU:0, one launch (start us, length us, event | category | flops | bytes accessed | tf_op | source)
XLA Modules:
  0.0 181.9 jit_solution(3520858285360557099)
XLA Ops:
  8.7 15.9 %all_gather.3 = bf16[16,2048]{1,0:T(8,128)(2,1)S(1)} all-gather(bf16[16,256]{1,0:T(8,128)(2,1)} %param.23), channel_id=1, replica_groups=mesh['ep'=4,'tp'=8] {'tp'}, dimensions={1}, use_global_device_ids=true | all-gather | bytes 73728 | tf_op jit(solution)/shard_map/all_gather | solution.py:100
  24.8 1.5 fusion.70
  26.4 1.5 fusion.73
  28.1 1.1 select_reduce_fusion
  31.8 5.6 %fusion.34 = f32[16,2,1,1024]{3,2,1,0:T(1,128)S(1)} fusion(bf16[16,2,1024,128]{3,2,1,0:T(8,128)(2,1)} %param.24, bf16[16,2,128,1]{2,1,0,3:T(2,128)(2,1)S(1)} %get-tuple-element.12), kind=kOutput, calls=%fused_computation.64 | convolution fusion | flops 8388608 | bytes 8527872 | tf_op jit(solution)/shard_map/shd,shld->shl/dot_general | solution.py:52
  38.8 4.6 %fusion.24 = f32[16,2,1,128]{3,2,1,0:T(1,128)S(1)} fusion(bf16[16,2,1024,128]{3,2,1,0:T(8,128)(2,1)} %param.25, bf16[16,2,1024,1]{2,1,0,3:T(2,128)(2,1)S(1)} %fusion.26), kind=kOutput, calls=%fused_computation.33 | convolution fusion | flops 8388608 | bytes 8470528 | tf_op jit(solution)/shard_map/shl,shld->shd/dot_general | solution.py:68
  44.7 31.4 %reduce-scatter.4.cloned.1.call-done = f32[16,256]{1,0:T(8,128)} async-done(((f32[16,2048]{1,0:T(8,128)}), f32[16,256]{1,0:T(8,128)}) %reduce-scatter.4.cloned.1.call-update) | async-done | bytes 16400 | tf_op jit(solution)/shard_map/reduce_scatter | solution.py:131
  76.9 4.8 %collective-permute-done = bf16[16,256]{1,0:T(8,128)(2,1)S(1)} collective-permute-done((bf16[16,256]{1,0:T(8,128)(2,1)S(1)}, bf16[16,256]{1,0:T(8,128)(2,1)S(1)}, u32[]{:S(2)}, u32[]{:S(2)}) %collective-permute-start) | collective-permute-done | bytes 8224 | tf_op jit(solution)/shard_map/ppermute | solution.py:26
  81.7 3.6 %collective-permute-start.4 = (bf16[16,256]{1,0:T(8,128)(2,1)S(1)}, bf16[16,256]{1,0:T(8,128)(2,1)S(1)}, u32[]{:S(2)}, u32[]{:S(2)}) collective-permute-start(bf16[16,256]{1,0:T(8,128)(2,1)S(1)} %add_convert_fusion), channel_id=1, source_target_pairs={{0,7},{1,0},{2,1},{3,2},{4,3},{5,4},{6,5},{7,6},{8,15},{9,8},{10,9... | collective-permute-start | bytes 24584 | tf_op jit(solution)/shard_map/ppermute | solution.py:29
  85.3 1.3 collective-permute-done.1
  87.4 3.6 %all-to-all-start.1 = ((bf16[4,8,4]{1,2,0:T(4,128)(2,1)}), bf16[4,8,4]{1,2,0:T(4,128)(2,1)S(1)}, u32[]{:S(2)}, u32[]{:S(2)}) async-start(bf16[4,8,4]{1,2,0:T(4,128)(2,1)} %copy.49), calls=%async_computation.2 | async-start | bytes 8192 | tf_op jit(solution)/shard_map/all_to_all | solution.py:154
  91.1 3.3 %collective-permute-start.5 = (bf16[16,256]{1,0:T(8,128)(2,1)S(1)}, bf16[16,256]{1,0:T(8,128)(2,1)S(1)}, u32[]{:S(2)}, u32[]{:S(2)}) collective-permute-start(bf16[16,256]{1,0:T(8,128)(2,1)S(1)} %collective-permute-done.4), channel_id=1, source_target_pairs={{0,7},{1,0},{2,1},{3,2},{4,3},{5,4},{6,5},{7,6},{8,15},{9,8},{10,9... | collective-permute-start | bytes 24584 | tf_op jit(solution)/shard_map/ppermute | solution.py:29
  94.4 1.3 collective-permute-done.5
  95.7 3.5 %collective-permute-start.6 = (bf16[16,256]{1,0:T(8,128)(2,1)S(1)}, bf16[16,256]{1,0:T(8,128)(2,1)S(1)}, u32[]{:S(2)}, u32[]{:S(2)}) collective-permute-start(bf16[16,256]{1,0:T(8,128)(2,1)S(1)} %collective-permute-done.5), channel_id=1, source_target_pairs={{0,7},{1,0},{2,1},{3,2},{4,3},{5,4},{6,5},{7,6},{8,15},{9,8},{10,9... | collective-permute-start | bytes 24584 | tf_op jit(solution)/shard_map/ppermute | solution.py:29
  99.3 1.3 collective-permute-done.6
  101.7 3.9 %all-to-all-start = ((bf16[4,8,2048]{2,1,0:T(8,128)(2,1)}), bf16[4,8,2048]{2,1,0:T(8,128)(2,1)S(1)}, u32[]{:S(2)}, u32[]{:S(2)}) async-start(bf16[4,8,2048]{2,1,0:T(8,128)(2,1)} %fusion), calls=%async_computation.1 | async-start | bytes 262144 | tf_op jit(solution)/shard_map/all_to_all | solution.py:153
  105.7 4.8 %all-to-all-done = bf16[4,8,2048]{2,1,0:T(8,128)(2,1)S(1)} async-done(((bf16[4,8,2048]{2,1,0:T(8,128)(2,1)}), bf16[4,8,2048]{2,1,0:T(8,128)(2,1)S(1)}, u32[]{:S(2)}, u32[]{:S(2)}) %all-to-all-start) | async-done | bytes 131104 | tf_op jit(solution)/shard_map/all_to_all | solution.py:153
  110.9 2.7 %fusion.4 = f32[32,2048]{1,0:T(8,128)} fusion(bf16[1,256,2048]{2,1,0:T(8,128)(2,1)S(1)} %copy-done, bf16[1,2048,256]{2,1,0:T(8,128)(2,1)} %param.41, bf16[4,8,2048]{2,1,0:T(8,128)(2,1)S(1)} %all-to-all-done, f32[32,256]{1,0:T(8,128)S(1)} %fusion.10, f32[32]{0:T(128)S(1)} %mul.185), kind=kOutput, calls=%fused_computation.7 | convolution fusion | flops 67166208 | bytes 2523264 | tf_op jit(solution)/shard_map/dot_general | solution.py:169
  113.6 3.0 %fusion.38 = f32[16,2048]{1,0:T(8,128)} fusion(bf16[256,2048]{1,0:T(8,128)(2,1)} %param.44, bf16[2048,256]{1,0:T(8,128)(2,1)} %param.43, f32[2048]{0:T(1024)S(1)} %copy-done.6, f32[16]{0:T(128)S(1)} %add_rsqrt_fusion.2, bf16[16,4096]{1,0:T(8,128)(2,1)S(1)} %constant_dynamic-update-slice_fusion, s32[]{:T(128)S(6)} %select_n.51), kind=kOutput, calls=%fused_computation.78 | convolution fusion | flops 33705984 | bytes 2302468 | tf_op jit(solution)/shard_map/dot_general | solution.py:159
  116.7 26.1 %reduce-scatter.6.cloned.1.call-done = f32[32,256]{1,0:T(8,128)} async-done(((f32[32,2048]{1,0:T(8,128)}), f32[32,256]{1,0:T(8,128)}) %reduce-scatter.6.cloned.1.call-update) | async-done | bytes 32784 | tf_op jit(solution)/shard_map/reduce_scatter | solution.py:171
  142.8 1.4 convert_bitcast_fusion
  144.2 3.7 %all-to-all-start.2 = ((bf16[4,8,256]{2,1,0:T(8,128)(2,1)}), bf16[4,8,256]{2,1,0:T(8,128)(2,1)S(1)}, u32[]{:S(2)}, u32[]{:S(2)}) async-start(bf16[4,8,256]{2,1,0:T(8,128)(2,1)} %convert_bitcast_fusion), calls=%async_computation.4 | async-start | bytes 32768 | tf_op jit(solution)/shard_map/all_to_all | solution.py:174
  147.8 26.0 %reduce-scatter.8.cloned.1.call-done = f32[16,256]{1,0:T(8,128)} async-done(((f32[16,2048]{1,0:T(8,128)}), f32[16,256]{1,0:T(8,128)}) %reduce-scatter.8.cloned.1.call-update) | async-done | bytes 16400 | tf_op jit(solution)/shard_map/reduce_scatter | solution.py:172
  173.8 1.5 fusion.5
  (104 shorter events, 10.3 us)
Async XLA Ops:
  7.2 103.7 %copy-start = (bf16[1,256,2048]{2,1,0:T(8,128)(2,1)S(1)}, bf16[1,256,2048]{2,1,0:T(8,128)(2,1)}, u32[]{:S(2)}) copy-start(bf16[1,256,2048]{2,1,0:T(8,128)(2,1)} %param.42) | copy-start | bytes 3145732
  7.2 31.3 %copy-start.5 = (f32[2048]{0:T(1024)S(1)}, f32[2048]{0:T(1024)}, u32[]{:S(2)}) copy-start(f32[2048]{0:T(1024)} %param.28) | copy-start | bytes 24580
  7.2 30.3 %copy-start.4 = (f32[16,2,1024]{2,1,0:T(2,128)S(1)}, f32[16,2,1024]{2,1,0:T(2,128)}, u32[]{:S(2)}) copy-start(f32[16,2,1024]{2,1,0:T(2,128)} %param.26) | copy-start | bytes 393220
  7.2 68.9 %reduce-scatter.4.cloned.1.call-start = ((), (), s32[]{:S(2)}) async-start(), calls=%async_computation.6 | async-start | bytes 147456 | tf_op jit(solution)/shard_map/reduce_scatter | solution.py:131
  31.0 12.3 %copy-start.11 = (f32[16,2]{0,1:T(2,128)}, f32[16,2]{0,1:T(2,128)S(1)}, u32[]{:S(2)}) copy-start(f32[16,2]{0,1:T(2,128)S(1)} %fusion.58) | copy-start | bytes 388
  37.5 38.6 %copy-start.8 = (bf16[16,256]{1,0:T(8,128)(2,1)S(1)}, bf16[16,256]{1,0:T(8,128)(2,1)}, u32[]{:S(2)}) copy-start(bf16[16,256]{1,0:T(8,128)(2,1)} %param.23) | copy-start | bytes 24580
  37.5 39.3 %copy-start.14 = (f32[16]{0:T(128)S(1)}, f32[16]{0:T(128)}, u32[]{:S(2)}) copy-start(f32[16]{0:T(128)} %param.38) | copy-start | bytes 196
  37.5 44.2 %copy-start.10 = (s32[16,2]{0,1:T(2,128)S(1)}, s32[16,2]{0,1:T(2,128)}, u32[]{:S(2)}) copy-start(s32[16,2]{0,1:T(2,128)} %param.37) | copy-start | bytes 388
  37.5 63.2 %copy-start.6 = (f32[2048]{0:T(1024)S(1)}, f32[2048]{0:T(1024)}, u32[]{:S(2)}) copy-start(f32[2048]{0:T(1024)} %param.35) | copy-start | bytes 24580
  37.9 72.7 %copy-start.2 = (bf16[1,2048,256]{2,1,0:T(8,128)(2,1)S(1)}, bf16[1,2048,256]{2,1,0:T(8,128)(2,1)}, u32[]{:S(2)}) copy-start(bf16[1,2048,256]{2,1,0:T(8,128)(2,1)} %param.40) | copy-start | bytes 3145732
  38.8 74.8 %copy-start.7 = (bf16[16,2,128]{2,1,0:T(2,128)(2,1)}, bf16[16,2,128]{2,1,0:T(2,128)(2,1)S(1)}, u32[]{:S(2)}) copy-start(bf16[16,2,128]{2,1,0:T(2,128)(2,1)S(1)} %convert_element_type.102) | copy-start | bytes 24580
  38.8 109.0 %copy-start.13 = (f32[256]{0:T(256)S(1)}, f32[256]{0:T(256)}, u32[]{:S(2)}) copy-start(f32[256]{0:T(256)} %param.45) | copy-start | bytes 3076
  76.9 4.9 %collective-permute-start = (bf16[16,256]{1,0:T(8,128)(2,1)S(1)}, bf16[16,256]{1,0:T(8,128)(2,1)S(1)}, u32[]{:S(2)}, u32[]{:S(2)}) collective-permute-start(bf16[16,256]{1,0:T(8,128)(2,1)S(1)} %add_convert_fusion), channel_id=1, source_target_pairs={{0,1},{1,2},{2,3},{3,4},{4,5},{5,6},{6,7},{7,0},{8,9},{9,10},{10,1... | collective-permute-start | bytes 24584 | tf_op jit(solution)/shard_map/ppermute | solution.py:26
  81.7 4.9 %collective-permute-start.1 = (bf16[16,256]{1,0:T(8,128)(2,1)S(1)}, bf16[16,256]{1,0:T(8,128)(2,1)S(1)}, u32[]{:S(2)}, u32[]{:S(2)}) collective-permute-start(bf16[16,256]{1,0:T(8,128)(2,1)S(1)} %collective-permute-done), channel_id=1, source_target_pairs={{0,1},{1,2},{2,3},{3,4},{4,5},{5,6},{6,7},{7,0},{8,9},{9,10},{10,1... | collective-permute-start | bytes 24584 | tf_op jit(solution)/shard_map/ppermute | solution.py:26
  81.7 9.3 %collective-permute-start.4 = (bf16[16,256]{1,0:T(8,128)(2,1)S(1)}, bf16[16,256]{1,0:T(8,128)(2,1)S(1)}, u32[]{:S(2)}, u32[]{:S(2)}) collective-permute-start(bf16[16,256]{1,0:T(8,128)(2,1)S(1)} %add_convert_fusion), channel_id=1, source_target_pairs={{0,7},{1,0},{2,1},{3,2},{4,3},{5,4},{6,5},{7,6},{8,15},{9,8},{10,9... | collective-permute-start | bytes 24584 | tf_op jit(solution)/shard_map/ppermute | solution.py:29
  86.6 7.7 %collective-permute-start.2 = (bf16[16,256]{1,0:T(8,128)(2,1)S(1)}, bf16[16,256]{1,0:T(8,128)(2,1)S(1)}, u32[]{:S(2)}, u32[]{:S(2)}) collective-permute-start(bf16[16,256]{1,0:T(8,128)(2,1)S(1)} %collective-permute-done.1), channel_id=1, source_target_pairs={{0,1},{1,2},{2,3},{3,4},{4,5},{5,6},{6,7},{7,0},{8,9},{9,10},{10,1... | collective-permute-start | bytes 24584 | tf_op jit(solution)/shard_map/ppermute | solution.py:26
  87.4 14.2 %all-to-all-start.1 = ((bf16[4,8,4]{1,2,0:T(4,128)(2,1)}), bf16[4,8,4]{1,2,0:T(4,128)(2,1)S(1)}, u32[]{:S(2)}, u32[]{:S(2)}) async-start(bf16[4,8,4]{1,2,0:T(4,128)(2,1)} %copy.49), calls=%async_computation.2 | async-start | bytes 8192 | tf_op jit(solution)/shard_map/all_to_all | solution.py:154
  91.1 4.6 %collective-permute-start.5 = (bf16[16,256]{1,0:T(8,128)(2,1)S(1)}, bf16[16,256]{1,0:T(8,128)(2,1)S(1)}, u32[]{:S(2)}, u32[]{:S(2)}) collective-permute-start(bf16[16,256]{1,0:T(8,128)(2,1)S(1)} %collective-permute-done.4), channel_id=1, source_target_pairs={{0,7},{1,0},{2,1},{3,2},{4,3},{5,4},{6,5},{7,6},{8,15},{9,8},{10,9... | collective-permute-start | bytes 24584 | tf_op jit(solution)/shard_map/ppermute | solution.py:29
  94.3 4.9 %collective-permute-start.3 = (bf16[16,256]{1,0:T(8,128)(2,1)S(1)}, bf16[16,256]{1,0:T(8,128)(2,1)S(1)}, u32[]{:S(2)}, u32[]{:S(2)}) collective-permute-start(bf16[16,256]{1,0:T(8,128)(2,1)S(1)} %collective-permute-done.2), channel_id=1, source_target_pairs={{0,1},{1,2},{2,3},{3,4},{4,5},{5,6},{6,7},{7,0},{8,9},{9,10},{10,1... | collective-permute-start | bytes 24584 | tf_op jit(solution)/shard_map/ppermute | solution.py:26
  95.7 4.9 %collective-permute-start.6 = (bf16[16,256]{1,0:T(8,128)(2,1)S(1)}, bf16[16,256]{1,0:T(8,128)(2,1)S(1)}, u32[]{:S(2)}, u32[]{:S(2)}) collective-permute-start(bf16[16,256]{1,0:T(8,128)(2,1)S(1)} %collective-permute-done.5), channel_id=1, source_target_pairs={{0,7},{1,0},{2,1},{3,2},{4,3},{5,4},{6,5},{7,6},{8,15},{9,8},{10,9... | collective-permute-start | bytes 24584 | tf_op jit(solution)/shard_map/ppermute | solution.py:29
  101.7 8.9 %all-to-all-start = ((bf16[4,8,2048]{2,1,0:T(8,128)(2,1)}), bf16[4,8,2048]{2,1,0:T(8,128)(2,1)S(1)}, u32[]{:S(2)}, u32[]{:S(2)}) async-start(bf16[4,8,2048]{2,1,0:T(8,128)(2,1)} %fusion), calls=%async_computation.1 | async-start | bytes 262144 | tf_op jit(solution)/shard_map/all_to_all | solution.py:153
  105.6 37.2 %reduce-scatter.6.cloned.1.call-start = ((), (), s32[]{:S(2)}) async-start(), calls=%async_computation.7 | async-start | bytes 294912 | tf_op jit(solution)/shard_map/reduce_scatter | solution.py:171
  113.6 60.2 %reduce-scatter.8.cloned.1.call-start = ((), (), s32[]{:S(2)}) async-start(), calls=%async_computation.8 | async-start | bytes 147456 | tf_op jit(solution)/shard_map/reduce_scatter | solution.py:172
  144.2 29.7 %all-to-all-start.2 = ((bf16[4,8,256]{2,1,0:T(8,128)(2,1)}), bf16[4,8,256]{2,1,0:T(8,128)(2,1)S(1)}, u32[]{:S(2)}, u32[]{:S(2)}) async-start(bf16[4,8,256]{2,1,0:T(8,128)(2,1)} %convert_bitcast_fusion), calls=%async_computation.4 | async-start | bytes 32768 | tf_op jit(solution)/shard_map/all_to_all | solution.py:174
  (4 other events, 27.5 us)
Sparse Core Ops, SparseCore 0:
  44.5 31.5 reduce-scatter.3
  113.7 29.0 reduce-scatter.5
  145.1 28.7 reduce-scatter.7
